TPU v7x, 256 devices: a whole 4x4x8 slice. The times are simulated.
256 devices in a mesh: sp: 32 (over z, x), tp: 8 (over y, core).
Axes of the slice: x: 4, y: 4, z: 8, core: 2. Of those that a mesh axis runs over, the one named last changes fastest.
Arguments:
- residual: bfloat16 [24576, 2048], P('sp'), may hold values from -6 to 6
- queries: bfloat16 [24576, 1024], P('sp', 'tp'), may hold values from -12 to 12
- keys: bfloat16 [24576, 512], P('sp', 'tp'), may hold values from -6 to 6
- values: bfloat16 [24576, 512], P('sp', 'tp'), may hold values from -36 to 36
- segments: int32 [24576], P('sp'), may hold values from 0 to 15, never falling along the last dimension, each value on 1 to 3072 neighbouring positions
- sink: float32 [16], P('tp'), may hold values from 3 to 7
- out_weight: bfloat16 [1024, 2048], replicated, may hold values from -0.1875 to 0.1875
- norm_gain_one: float32 [2048], replicated, may hold values from 0.1 to 1.9
- group: int32 [24576], P('sp'), may hold values from 0 to 3, as said below
- member: int32 [24576, 2], P('sp'), may hold values from 0 to 7, as said below
- route_weight: float32 [24576, 2], P('sp'), may hold values from 0.25 to 1
- gate_weight: bfloat16 [32, 2048, 1024], P('sp', None, 'tp'), may hold values from -0.125 to 0.125
- up_weight: bfloat16 [32, 2048, 1024], P('sp', None, 'tp'), may hold values from -0.125 to 0.125
- down_weight: bfloat16 [32, 1024, 2048], P('sp', None, 'tp'), may hold values from -0.1875 to 0.1875
- norm_gain_two: float32 [2048], P('tp'), may hold values from 0.1 to 1.9
Outputs:
- output: bfloat16 [24576, 2048], P('sp', 'tp')
Inputs may be any that keep to these rules, and one draw needn't show every extreme that they name: In every aligned block of 96 rows no expert (group * 8 + member) is named by more than 12 rows, and one expert, the same in all blocks of a draw, is named by exactly 12 rows of every block. `member`: the 2 members of a row differ.
All inputs are finite; a program needn't handle non-finite values.
Results may differ from a plain program's by a relative error of at most 0.0059.
Values may be sent and summed in bfloat16 or wider, within the bound.
No kernel may reach another device: no remote copies, remote signals or barrier semaphores. Data moves between devices by JAX's collectives and lax.ppermute only.
A program may use at most 128 MiB of HBM per device.

v0:
```python
import math
import jax
import jax.numpy as jnp
from jax import lax
from jax.sharding import PartitionSpec as P

HEAD_DIM = 64
HALF = 128
PER_GROUP = 8
ALPHA = 2.0**0.25
EPS = 1e-05


def with_halo(block, sides, width):
    for axis, dim in sides:
        count = lax.axis_size(axis)
        forward = [(i, i + 1) for i in range(count - 1)]
        backward = [(target, source) for source, target in forward]
        low = lax.ppermute(
            lax.slice_in_dim(block, block.shape[dim] - width, None, axis=dim), axis, forward
        )
        high = lax.ppermute(lax.slice_in_dim(block, 0, width, axis=dim), axis, backward)
        block = jnp.concatenate([low, block, high], axis=dim)
    return block


def copy_for_each(x, axis):
    copies = jnp.broadcast_to(x, (lax.axis_size(axis), *x.shape))
    return lax.all_to_all(copies, axis, split_axis=0, concat_axis=0, tiled=True)


def joined_along(pieces, dim):
    pieces = jnp.moveaxis(pieces, 0, dim)
    lengths = pieces.shape
    return pieces.reshape(*lengths[:dim], lengths[dim] * lengths[dim + 1], *lengths[dim + 2 :])


def gather_directly(x, axis, dim):
    pieces = copy_for_each(x, axis)
    return joined_along(pieces, dim)


def taken_together(x, axis):
    everything = copy_for_each(x, axis)
    return jnp.sum(everything, axis=0)


def packed_total(arrays, axis):
    ends = [0]
    for a in arrays:
        ends.append(ends[-1] + a.size)
    subtotal = taken_together(jnp.concatenate([a.ravel() for a in arrays]), axis)
    return tuple((subtotal[b:e].reshape(a.shape) for a, b, e in zip(arrays, ends, ends[1:])))


def layer_norm(summed, norm_gain):
    mean_value = jnp.mean(summed, -1, keepdims=True)
    variance = jnp.mean(jnp.square(summed - mean_value), -1, keepdims=True)
    return ((summed - mean_value) * lax.rsqrt(variance + EPS) * norm_gain).astype(jnp.bfloat16)


def shards(
    residual,
    queries,
    keys,
    values,
    segments,
    sink,
    out_weight,
    norm_gain_one,
    group,
    member,
    route_weight,
    gate_weight,
    up_weight,
    down_weight,
    norm_gain_two,
):
    row_count = queries.shape[0]
    sp_size = lax.axis_size("sp")
    tp_size = lax.axis_size("tp")
    kv_local = keys.shape[1] // HEAD_DIM
    heads_local = queries.shape[1] // HEAD_DIM
    group_size = heads_local // kv_local
    seq_total = row_count * sp_size
    seq_start = lax.axis_index("sp") * row_count
    joined = jnp.concatenate([keys, values], axis=1)
    padded, seg_padded = (
        with_halo(joined, (("sp", 0),), HALF),
        with_halo(segments, (("sp", 0),), HALF),
    )
    query_block = math.gcd(row_count, 512)
    key_span = query_block + 2 * HALF
    offsets = jnp.arange(key_span)[None, :] - HALF - jnp.arange(query_block)[:, None]
    in_band = jnp.abs(offsets) <= HALF
    sink_heads = sink.reshape(kv_local, group_size, 1, 1)
    query_heads = queries.reshape(row_count, kv_local, group_size, HEAD_DIM)
    key_cols = kv_local * HEAD_DIM
    pieces = []
    for number in range(row_count // query_block):
        row_low = number * query_block
        query_rows = query_heads[row_low : row_low + query_block]
        kv_rows = padded[row_low : row_low + key_span]
        key_part = kv_rows[:, :key_cols].reshape(key_span, kv_local, HEAD_DIM)
        value_part = kv_rows[:, key_cols:].reshape(key_span, kv_local, HEAD_DIM)
        key_place = seq_start + row_low - HALF + jnp.arange(key_span)
        inside = (key_place >= 0) & (key_place < seq_total)
        same_doc = (
            segments[row_low : row_low + query_block, None]
            == seg_padded[None, row_low : row_low + key_span]
        )
        allowed = in_band & same_doc & inside[None, :]
        scores = jnp.einsum(
            "qkgd,ckd->kgqc", query_rows, key_part, preferred_element_type=jnp.float32
        ) * HEAD_DIM ** (-0.5)
        masked = jnp.where(allowed, scores, -1e30)
        peak = jnp.maximum(jnp.max(masked, -1, keepdims=True), sink_heads)
        raised = jnp.where(allowed, jnp.exp(masked - peak), 0.0)
        denominator = jnp.sum(raised, -1, keepdims=True) + jnp.exp(sink_heads - peak)
        weights = (raised / denominator).astype(jnp.bfloat16)
        attended_part = jnp.einsum(
            "kgqc,ckd->qkgd", weights, value_part, preferred_element_type=jnp.float32
        )
        pieces.append(
            attended_part.reshape(query_block, heads_local * HEAD_DIM).astype(jnp.bfloat16)
        )
    attended = jnp.concatenate(pieces, 0)
    width = out_weight.shape[1]
    weight_rows = out_weight
    mixed = jnp.dot(
        gather_directly(attended, "tp", 1), weight_rows, preferred_element_type=jnp.float32
    )
    pre_one = ALPHA * residual.astype(jnp.float32) + mixed
    normed = layer_norm(pre_one, norm_gain_one)
    experts_local = gate_weight.shape[0]
    expert_count = experts_local * sp_size
    picks_count = member.shape[1]
    block_rows = row_count // tp_size
    capacity = max(2, block_rows // 8)
    expert_ids = (group[:, None] * PER_GROUP + member).reshape(tp_size, block_rows * picks_count)
    onehot_table = (expert_ids[:, :, None] == jnp.arange(expert_count)[None, None, :]).astype(
        jnp.int32
    )
    ranks = jnp.sum((jnp.cumsum(onehot_table, 1) - 1) * onehot_table, 2)
    owner = expert_ids // experts_local
    local_ids = expert_ids % experts_local
    block_ids = jnp.arange(tp_size)[:, None]
    slot_all = ((local_ids * sp_size + owner) * tp_size + block_ids) * capacity + ranks
    copy_rows = (
        jnp.arange(row_count * picks_count).reshape(tp_size, block_rows * picks_count)
        // picks_count
    )
    extended = jnp.concatenate([normed, jnp.zeros((1, width), jnp.bfloat16)], 0)
    tp_place = lax.axis_index("tp")
    slot_own_base = (local_ids * sp_size + owner) * capacity + ranks
    own_slots = lax.dynamic_index_in_dim(slot_own_base, tp_place, 0, keepdims=False)
    own_rows = lax.dynamic_index_in_dim(copy_rows, tp_place, 0, keepdims=False)
    slot_count = experts_local * sp_size * capacity
    source = jnp.full((slot_count,), row_count, jnp.int32).at[own_slots].set(own_rows)
    outgoing = extended[source].reshape(experts_local, sp_size, capacity, width)
    received = lax.all_to_all(outgoing, "sp", split_axis=1, concat_axis=1, tiled=True)
    arrived = lax.all_gather(received, "tp", axis=2, tiled=True)
    expert_rows = arrived.reshape(experts_local, sp_size * tp_size * capacity, width)
    gate_part = jnp.einsum(
        "esd,edf->esf", expert_rows, gate_weight, preferred_element_type=jnp.float32
    )
    up_part = jnp.einsum("esd,edf->esf", expert_rows, up_weight, preferred_element_type=jnp.float32)
    hidden = (jax.nn.silu(gate_part) * up_part).astype(jnp.bfloat16)
    column_width = down_weight.shape[2]
    weight_rows = down_weight
    produced = jnp.einsum(
        "esf,efc->esc",
        lax.all_gather(hidden, "tp", axis=2, tiled=True),
        weight_rows,
        preferred_element_type=jnp.float32,
    ).astype(jnp.bfloat16)
    returned = lax.all_to_all(
        produced.reshape(experts_local, sp_size, tp_size * capacity, column_width),
        "sp",
        split_axis=1,
        concat_axis=1,
        tiled=True,
    )
    result_rows = returned.reshape(-1, column_width)
    picked = result_rows[slot_all.reshape(row_count, picks_count)]
    combined = jnp.sum(route_weight[:, :, None] * picked.astype(jnp.float32), 1)
    column_start = lax.axis_index("tp") * column_width
    normed_part = lax.dynamic_slice_in_dim(normed, column_start, column_width, 1)
    pre_two = ALPHA * normed_part.astype(jnp.float32) + combined
    sums, squares = packed_total((jnp.sum(pre_two, -1), jnp.sum(pre_two * pre_two, -1)), "tp")
    mean_value = (sums / width)[:, None]
    variance = (squares / width)[:, None] - mean_value * mean_value
    return ((pre_two - mean_value) * lax.rsqrt(variance + EPS) * norm_gain_two).astype(jnp.bfloat16)


def solution(mesh):
    in_specs = (
        P("sp", None),
        P("sp", "tp"),
        P("sp", "tp"),
        P("sp", "tp"),
        P("sp"),
        P("tp"),
        P(),
        P(),
        P("sp"),
        P("sp", None),
        P("sp", None),
        P("sp", None, "tp"),
        P("sp", None, "tp"),
        P("sp", None, "tp"),
        P("tp"),
    )
    out_specs = P("sp", "tp")
    return jax.shard_map(shards, mesh=mesh, in_specs=in_specs, out_specs=out_specs, check_vma=False)
```

profile of v0, /device:TPU:1, one launch (start us, length us, event | category | flops | bytes accessed | tf_op | source)
XLA Modules:
  0.0 366.8 jit_solution(6680165087132534622)
XLA Ops:
  7.4 3.9 %collective-permute-start.1 = (s32[128]{0:T(128)S(1)}, s32[128]{0:T(128)S(1)}, u32[]{:S(2)}, u32[]{:S(2)}) collective-permute-start(s32[128]{0:T(128)S(1)} %get-tuple-element.16), channel_id=1, source_target_pairs={{0,8},{8,16},{16,24},{24,32},{32,40},{40,48},{48,56},{56,64},{64,7... | collective-permute-start | bytes 1544 | tf_op jit(solution)/shard_map/ppermute | solution.py:19
  14.4 4.0 %collective-permute-start = (bf16[128,128]{0,1:T(8,128)(2,1)S(1)}, bf16[128,128]{0,1:T(8,128)(2,1)S(1)}, u32[]{:S(2)}, u32[]{:S(2)}) collective-permute-start(bf16[128,128]{0,1:T(8,128)(2,1)S(1)} %get-tuple-element.7), channel_id=1, source_target_pairs={{0,8},{8,16},{16,24},{24,32},{32,40},{40,48},{48,56},{56,64},{64,7... | collective-permute-start | bytes 98312 | tf_op jit(solution)/shard_map/ppermute | solution.py:19
  29.7 6.0 %all-to-all-start = ((bf16[8,768,128]{1,2,0:T(8,128)(2,1)}), bf16[8,768,128]{1,2,0:T(8,128)(2,1)S(1)}, u32[]{:S(2)}, u32[]{:S(2)}) async-start(bf16[8,768,128]{1,2,0:T(8,128)(2,1)} %broadcast_in_dim.73), calls=%async_computation | async-start | bytes 3145728 | tf_op jit(solution)/shard_map/all_to_all | solution.py:29
  35.7 4.6 %reduce-window.6 = s32[8,32,2,128]{3,1,2,0:T(8,128)S(1)} reduce-window(s32[8,32,2,128]{3,1,2,0:T(8,128)S(1)} %copy_bitcast_fusion, s32[]{:T(128)} %constant.104.clone.1), window={size=1x1x1x128 pad=0_0x0_0x0_0x127_0}, to_apply=%region_8.9 | reduce-window | flops 8323072 | bytes 524292 | tf_op jit(solution)/shard_map/reduce-window
  42.4 13.9 %all-to-all-done = bf16[8,768,128]{1,2,0:T(8,128)(2,1)S(1)} async-done(((bf16[8,768,128]{1,2,0:T(8,128)(2,1)}), bf16[8,768,128]{1,2,0:T(8,128)(2,1)S(1)}, u32[]{:S(2)}, u32[]{:S(2)}) %all-to-all-start) | async-done | bytes 1572896 | tf_op jit(solution)/shard_map/all_to_all | solution.py:29
  56.3 7.3 %fusion.69 = (f32[768]{0:T(1024)S(1)}, f32[768,2048]{1,0:T(8,128)S(1)}) fusion(bf16[768,1024]{0,1:T(8,128)(2,1)S(1)} %bitcast.123, bf16[1024,2048]{1,0:T(8,128)(2,1)} %param.21, bf16[768,2048]{1,0:T(8,128)(2,1)} %param.15), kind=kOutput, calls=%fused_computation.143 | convolution fusion | flops 3227516160 | bytes 15207424 | tf_op jit(solution)/shard_map/dot_general | solution.py:130
  67.0 2.0 concatenate.32
  69.1 7.4 %gather_fusion = bf16[384,2048]{1,0:T(8,128)(2,1)} fusion(bf16[769,2048]{1,0:T(8,128)(2,1)} %concatenate.32, s32[1024]{0:T(1024)S(1)} %pad_clamp_fusion.1), kind=kCustom, calls=%fused_computation | custom fusion | bytes 3147264 | tf_op jit(solution)/shard_map/gather | solution.py:160
  76.4 2.4 reshape.420
  78.8 64.7 %all_to_all.21 = bf16[1,32,12,2048]{3,2,0,1:T(8,128)(2,1)S(1)} all-to-all(bf16[1,32,12,2048]{3,2,0,1:T(8,128)(2,1)S(1)} %bitcast.122), channel_id=1, replica_groups=mesh['sp'=32,'tp'=8] {'sp'}, dimensions={1} | all-to-all | bytes 3145728 | tf_op jit(solution)/shard_map/all_to_all | solution.py:161
  143.5 2.0 copy.96
  145.8 67.6 %all-gather.4.cloned.1.call-done = bf16[1,32,96,2048]{3,1,0,2:T(8,128)(2,1)} async-done(((bf16[1,32,12,2048]{3,1,0,2:T(8,128)(2,1)}), bf16[1,32,96,2048]{3,1,0,2:T(8,128)(2,1)}) %all-gather.4.cloned.1.call-update) | async-done | bytes 12582928 | tf_op jit(solution)/shard_map/all_gather | solution.py:162
  213.4 11.7 %copy.97 = bf16[1,32,96,2048]{3,2,1,0:T(8,128)(2,1)S(1)} copy(bf16[1,32,96,2048]{3,1,0,2:T(8,128)(2,1)} %all-gather.4.cloned.1.call-done) | data formatting | bytes 25165824 | tf_op jit(solution)/shard_map/all_gather | solution.py:162
  225.2 3.5 fusion.12
  228.7 4.5 %fusion = bf16[3072,128]{1,0:T(8,128)(2,1)} fusion(bf16[3072,2048]{1,0:T(8,128)(2,1)S(1)} %bitcast.121, f32[3072,128]{1,0:T(8,128)S(1)} %fusion.12, bf16[1,2048,128]{2,1,0:T(8,128)(2,1)S(1)} %copy-done.10), kind=kOutput, calls=%fused_computation.8 | convolution fusion | flops 1612972032 | bytes 15466496 | tf_op jit(solution)/shard_map/esd,edf->esf/dot_general | solution.py:167
  233.2 47.5 %all-gather.6.cloned.1.call-done = bf16[3072,1024]{1,0:T(8,128)(2,1)} async-done(((bf16[3072,128]{1,0:T(8,128)(2,1)}), bf16[3072,1024]{1,0:T(8,128)(2,1)}) %all-gather.6.cloned.1.call-update) | async-done | bytes 6291472 | tf_op jit(solution)/shard_map/all_gather | solution.py:173
  280.8 5.7 %convolution_convert_fusion = bf16[3072,256]{1,0:T(8,128)(2,1)} fusion(bf16[3072,1024]{1,0:T(8,128)(2,1)} %all-gather.6.cloned.1.call-done, bf16[1,1024,256]{2,1,0:T(8,128)(2,1)S(1)} %copy-done), kind=kOutput, calls=%fused_computation.6 | convolution fusion | flops 1611399168 | bytes 8388608 | tf_op jit(solution)/shard_map/esf,efc->esc/dot_general | solution.py:171
  286.5 9.9 %all-to-all-start.2 = ((bf16[1,32,96,256]{3,2,0,1:T(8,128)(2,1)}), bf16[1,32,96,256]{3,2,0,1:T(8,128)(2,1)S(1)}, u32[]{:S(2)}, u32[]{:S(2)}) async-start(bf16[1,32,96,256]{3,2,0,1:T(8,128)(2,1)} %bitcast.124), calls=%async_computation.2 | async-start | bytes 3145728 | tf_op jit(solution)/shard_map/all_to_all | solution.py:177
  297.6 36.4 %all-to-all-done.2 = bf16[1,32,96,256]{3,2,0,1:T(8,128)(2,1)S(1)} async-done(((bf16[1,32,96,256]{3,2,0,1:T(8,128)(2,1)}), bf16[1,32,96,256]{3,2,0,1:T(8,128)(2,1)S(1)}, u32[]{:S(2)}, u32[]{:S(2)}) %all-to-all-start.2) | async-done | bytes 1572896 | tf_op jit(solution)/shard_map/all_to_all | solution.py:177
  334.0 5.3 %gather_fusion.1 = bf16[1536,256]{1,0:T(8,128)(2,1)} fusion(bf16[3072,256]{1,0:T(8,128)(2,1)S(1)} %bitcast.119, s32[2048]{0:T(1024)S(1)} %pad_clamp_fusion), kind=kCustom, calls=%fused_computation.1 | custom fusion | bytes 1579008 | tf_op jit(solution)/shard_map/gather | solution.py:185
  339.3 2.2 reshape.458
  341.5 4.2 %multiply_reduce_fusion.1 = f32[768,256]{1,0:T(8,128)S(1)} fusion(f32[768,2,256]{2,1,0:T(2,128)S(1)} %reshape.458, f32[768,2]{1,0:T(8,128)S(1)} %copy.89), kind=kLoop, calls=%fused_computation.9 | loop fusion | flops 589824 | bytes 2365440 | tf_op jit(solution)/shard_map/reduce_sum | solution.py:186
  347.1 10.8 %all_to_all.22 = f32[8,1,1536]{2,1,0:T(1,128)S(1)} all-to-all(f32[8,1,1536]{2,1,0:T(1,128)S(1)} %broadcast_in_dim.77), channel_id=1, replica_groups=mesh['sp'=32,'tp'=8] {'tp'}, dimensions={0} | all-to-all | bytes 98304 | tf_op jit(solution)/shard_map/all_to_all | solution.py:29
  357.9 2.0 multiply_convert_fusion.1
  (99 shorter events, 23.1 us)
Async XLA Ops:
  6.5 274.2 %copy-start = (bf16[1,1024,256]{2,1,0:T(8,128)(2,1)S(1)}, bf16[1,1024,256]{2,1,0:T(8,128)(2,1)}, u32[]{:S(2)}) copy-start(bf16[1,1024,256]{2,1,0:T(8,128)(2,1)} %param.28) | copy-start | bytes 1572868
  6.5 18.0 %copy-start.4 = (s32[768]{0:T(1024)S(1)}, s32[768]{0:T(1024)}, u32[]{:S(2)}) copy-start(s32[768]{0:T(1024)} %param.19) | copy-start | bytes 9220
  6.5 18.8 %copy-start.2 = (bf16[768,64]{0,1:T(8,128)(2,1)S(1)}, bf16[768,64]{0,1:T(8,128)(2,1)}, u32[]{:S(2)}) copy-start(bf16[768,64]{0,1:T(8,128)(2,1)} %param.17) | copy-start | bytes 294916
  7.4 17.2 %collective-permute-start.1 = (s32[128]{0:T(128)S(1)}, s32[128]{0:T(128)S(1)}, u32[]{:S(2)}, u32[]{:S(2)}) collective-permute-start(s32[128]{0:T(128)S(1)} %get-tuple-element.16), channel_id=1, source_target_pairs={{0,8},{8,16},{16,24},{24,32},{32,40},{40,48},{48,56},{56,64},{64,7... | collective-permute-start | bytes 1544 | tf_op jit(solution)/shard_map/ppermute | solution.py:19
  11.3 13.3 %collective-permute-start.3 = (s32[128]{0:T(128)S(1)}, s32[128]{0:T(128)S(1)}, u32[]{:S(2)}, u32[]{:S(2)}) collective-permute-start(s32[128]{0:T(128)S(1)} %get-tuple-element.17), channel_id=1, source_target_pairs={{8,0},{16,8},{24,16},{32,24},{40,32},{48,40},{56,48},{64,56},{72,6... | collective-permute-start | bytes 1544 | tf_op jit(solution)/shard_map/ppermute | solution.py:22
  14.4 11.7 %copy-start.7 = (f32[2]{0:T(128)S(1)}, f32[2]{0:T(128)}, u32[]{:S(2)}) copy-start(f32[2]{0:T(128)} %param.20) | copy-start | bytes 28
  14.4 11.3 %collective-permute-start = (bf16[128,128]{0,1:T(8,128)(2,1)S(1)}, bf16[128,128]{0,1:T(8,128)(2,1)S(1)}, u32[]{:S(2)}, u32[]{:S(2)}) collective-permute-start(bf16[128,128]{0,1:T(8,128)(2,1)S(1)} %get-tuple-element.7), channel_id=1, source_target_pairs={{0,8},{8,16},{16,24},{24,32},{32,40},{40,48},{48,56},{56,64},{64,7... | collective-permute-start | bytes 98312 | tf_op jit(solution)/shard_map/ppermute | solution.py:19
  18.4 7.9 %collective-permute-start.2 = (bf16[128,128]{0,1:T(8,128)(2,1)S(1)}, bf16[128,128]{0,1:T(8,128)(2,1)S(1)}, u32[]{:S(2)}, u32[]{:S(2)}) collective-permute-start(bf16[128,128]{0,1:T(8,128)(2,1)S(1)} %get-tuple-element.8), channel_id=1, source_target_pairs={{8,0},{16,8},{24,16},{32,24},{40,32},{48,40},{56,48},{64,56},{72,6... | collective-permute-start | bytes 98312 | tf_op jit(solution)/shard_map/ppermute | solution.py:22
  25.7 1.6 copy-start.3
  29.7 26.6 %all-to-all-start = ((bf16[8,768,128]{1,2,0:T(8,128)(2,1)}), bf16[8,768,128]{1,2,0:T(8,128)(2,1)S(1)}, u32[]{:S(2)}, u32[]{:S(2)}) async-start(bf16[8,768,128]{1,2,0:T(8,128)(2,1)} %broadcast_in_dim.73), calls=%async_computation | async-start | bytes 3145728 | tf_op jit(solution)/shard_map/all_to_all | solution.py:29
  35.7 177.7 %all-gather.4.cloned.1.call-start = ((), (), s32[]{:S(2)}) async-start(), calls=%async_computation.4 | async-start | bytes 14155776 | tf_op jit(solution)/shard_map/all_gather | solution.py:162
  63.7 0.8 copy-start.5
  65.3 1.7 copy-start.1
  145.5 79.6 %copy-start.9 = (bf16[1,2048,128]{2,1,0:T(8,128)(2,1)S(1)}, bf16[1,2048,128]{2,1,0:T(8,128)(2,1)}, u32[]{:S(2)}) copy-start(bf16[1,2048,128]{2,1,0:T(8,128)(2,1)} %param.26) | copy-start | bytes 1572868
  145.5 135.3 %all-gather.6.cloned.1.call-start = ((), (), s32[]{:S(2)}) async-start(), calls=%async_computation.5 | async-start | bytes 7077888 | tf_op jit(solution)/shard_map/all_gather | solution.py:173
  225.1 3.6 copy-start.10
  286.5 10.9 %copy-start.6 = (f32[768,2]{0,1:T(2,128)S(1)}, f32[768,2]{0,1:T(2,128)}, u32[]{:S(2)}) copy-start(f32[768,2]{0,1:T(2,128)} %param.25) | copy-start | bytes 18436
  286.5 47.5 %all-to-all-start.2 = ((bf16[1,32,96,256]{3,2,0,1:T(8,128)(2,1)}), bf16[1,32,96,256]{3,2,0,1:T(8,128)(2,1)S(1)}, u32[]{:S(2)}, u32[]{:S(2)}) async-start(bf16[1,32,96,256]{3,2,0,1:T(8,128)(2,1)} %bitcast.124), calls=%async_computation.2 | async-start | bytes 3145728 | tf_op jit(solution)/shard_map/all_to_all | solution.py:177
  339.3 18.6 %copy-start.8 = (f32[256]{0:T(256)S(1)}, f32[256]{0:T(256)}, u32[]{:S(2)}) copy-start(f32[256]{0:T(256)} %param.29) | copy-start | bytes 3076
Sparse Core Ops, SparseCore 0:
  145.6 67.7 all-gather.3
  233.3 47.3 all-gather.5
where the time goes:
time: 368 us; the launch traced here: 367 us
  waiting for transfers between devices  166 us (45%)
  blocking collectives  75.4 us (20%)
  local copies, waits for them, and re-layouts  44.9 us (12%)
  starting transfers between devices  26.7 us (7%)
  matrix products  23.2 us (6%)
  other arithmetic  17 us (5%)
  between operations  14 us (4%)
    all_gather x1, waiting for transfers between devices, shards(): arrived = lax.all_gather(received, 'tp', axis=2, tiled=True)  67.6 us
    all_to_all x1, blocking collectives, shards(): lax.all_to_all(outgoing, 'sp', split_axis=1, concat_axis=1, tiled=True)  64.7 us
    all_gather x1, waiting for transfers between devices, shards(): lax.all_gather(hidden, 'tp', axis=2, tiled=True)  47.5 us
    all_to_all x1, waiting for transfers between devices, shards(): lax.all_to_all(produced.reshape(experts_local, sp_size, tp_size * capacit...  36.4 us
    all_to_all x1, waiting for transfers between devices, copy_for_each(): return lax.all_to_all(copies, axis, split_axis=0, concat_axis=0, tiled=True)  13.9 us
    all_gather x1, local copies, waits for them, and re-layouts, shards(): arrived = lax.all_gather(received, 'tp', axis=2, tiled=True)  11.7 us
    all_to_all x1, blocking collectives, copy_for_each(): return lax.all_to_all(copies, axis, split_axis=0, concat_axis=0, tiled=True)  10.8 us
    all_to_all x1, starting transfers between devices, shards(): lax.all_to_all(produced.reshape(experts_local, sp_size, tp_size * capacit...  9.93 us
  transfers between devices with their start and end apart: 8, of which 4 were waited for; matrix products, arithmetic and copies ran while one was open for 4% of the time, Pallas kernels for 0%

commit v1 on v0

--- a/solution.py
+++ b/solution.py
@@ -159,7 +159,9 @@
     source = jnp.full((slot_count,), row_count, jnp.int32).at[own_slots].set(own_rows)
     outgoing = extended[source].reshape(experts_local, sp_size, capacity, width)
     received = lax.all_to_all(outgoing, "sp", split_axis=1, concat_axis=1, tiled=True)
-    arrived = lax.all_gather(received, "tp", axis=2, tiled=True)
+    arrived = jnp.concatenate(
+        lax.all_to_all(jnp.stack([received] * lax.axis_size("tp")), "tp", 0, 0), axis=2
+    )
     expert_rows = arrived.reshape(experts_local, sp_size * tp_size * capacity, width)
     gate_part = jnp.einsum(
         "esd,edf->esf", expert_rows, gate_weight, preferred_element_type=jnp.float32

time: 368 us -> 482 us (1.31)
  blocking collectives: 75.4 us -> 221 us
  waiting for transfers between devices: 166 us -> 94.7 us
  local copies, waits for them, and re-layouts: 44.9 us -> 79.8 us
    all_to_all x0 -> x1, blocking collectives: none -> 145 us  [shards(): lax.all_to_all(jnp.stack([received] * lax.axis_size('tp')), 'tp', 0, 0)]
    all_gather x1 -> x0, waiting for transfers between devices: 67.6 us -> none  [shards(): arrived = lax.all_gather(received, 'tp', axis=2, tiled=True)]
    another operation x2 -> x4, local copies, waits for them, and re-layouts: 0.01 us -> 26.2 us
    reshape x0 -> x1, local copies, waits for them, and re-layouts: none -> 21.1 us  [shards(): jnp.concatenate(lax.all_to_all(jnp.stack([received] * lax.axis_size('tp')...]
    all_gather x1 -> x0, local copies, waits for them, and re-layouts: 11.7 us -> none  [shards(): arrived = lax.all_gather(received, 'tp', axis=2, tiled=True)]
  transfers between devices with their start and end apart: 8 -> 7, of which waited for: 4 -> 3; matrix products, arithmetic and copies ran while one was open for 4% -> 3% of each run, Pallas kernels for 0% -> 0%
where the time goes in v1:
time: 482 us; the launch traced here: 480 us
  blocking collectives  221 us (46%)
  waiting for transfers between devices  94.7 us (20%)
  local copies, waits for them, and re-layouts  79.8 us (17%)
  matrix products  27.4 us (6%)
  starting transfers between devices  26.4 us (5%)
  other arithmetic  17 us (4%)
  between operations  13.9 us (3%)
    all_to_all x1, blocking collectives, shards(): lax.all_to_all(jnp.stack([received] * lax.axis_size('tp')), 'tp', 0, 0)  145 us
    all_to_all x1, blocking collectives, shards(): lax.all_to_all(outgoing, 'sp', split_axis=1, concat_axis=1, tiled=True)  64.7 us
    all_gather x1, waiting for transfers between devices, shards(): lax.all_gather(hidden, 'tp', axis=2, tiled=True)  44.3 us
    all_to_all x1, waiting for transfers between devices, shards(): lax.all_to_all(produced.reshape(experts_local, sp_size, tp_size * capacit...  36.4 us
    reshape x1, local copies, waits for them, and re-layouts, shards(): jnp.concatenate(lax.all_to_all(jnp.stack([received] * lax.axis_size('tp')...  21.1 us
    another operation x3, local copies, waits for them, and re-layouts  20 us
    all_to_all x1, waiting for transfers between devices, copy_for_each(): return lax.all_to_all(copies, axis, split_axis=0, concat_axis=0, tiled=True)  13.9 us
    all_to_all x1, blocking collectives, copy_for_each(): return lax.all_to_all(copies, axis, split_axis=0, concat_axis=0, tiled=True)  10.8 us
  transfers between devices with their start and end apart: 7, of which 3 were waited for; matrix products, arithmetic and copies ran while one was open for 3% of the time, Pallas kernels for 0%

profile of v1, /device:TPU:1, one launch (start us, length us, event | category | flops | bytes accessed | tf_op | source)
XLA Modules:
  0.0 480.2 jit_solution(9906472027228850505)
XLA Ops:
  7.4 3.9 collective-permute-start.1
  14.4 4.0 collective-permute-start
  29.7 6.0 %all-to-all-start = ((bf16[8,768,128]{1,2,0:T(8,128)(2,1)}), bf16[8,768,128]{1,2,0:T(8,128)(2,1)S(1)}, u32[]{:S(2)}, u32[]{:S(2)}) async-start(bf16[8,768,128]{1,2,0:T(8,128)(2,1)} %broadcast_in_dim.73), calls=%async_computation | async-start | bytes 3145728 | tf_op jit(solution)/shard_map/all_to_all | solution.py:29
  35.7 4.6 reduce-window.6
  42.4 13.9 %all-to-all-done = bf16[8,768,128]{1,2,0:T(8,128)(2,1)S(1)} async-done(((bf16[8,768,128]{1,2,0:T(8,128)(2,1)}), bf16[8,768,128]{1,2,0:T(8,128)(2,1)S(1)}, u32[]{:S(2)}, u32[]{:S(2)}) %all-to-all-start) | async-done | bytes 1572896 | tf_op jit(solution)/shard_map/all_to_all | solution.py:29
  56.3 7.3 %fusion.69 = (f32[768]{0:T(1024)S(1)}, f32[768,2048]{1,0:T(8,128)S(1)}) fusion(bf16[768,1024]{0,1:T(8,128)(2,1)S(1)} %bitcast.124, bf16[1024,2048]{1,0:T(8,128)(2,1)} %param.21, bf16[768,2048]{1,0:T(8,128)(2,1)} %param.15), kind=kOutput, calls=%fused_computation.143 | convolution fusion | flops 3227516160 | bytes 15207424 | tf_op jit(solution)/shard_map/dot_general | solution.py:130
  67.0 2.0 concatenate.32
  69.1 7.4 %gather_fusion = bf16[384,2048]{1,0:T(8,128)(2,1)} fusion(bf16[769,2048]{1,0:T(8,128)(2,1)} %concatenate.32, s32[1024]{0:T(1024)S(1)} %pad_clamp_fusion.1), kind=kCustom, calls=%fused_computation | custom fusion | bytes 3147264 | tf_op jit(solution)/shard_map/gather | solution.py:160
  76.4 2.4 reshape.425
  78.8 64.7 %all_to_all.29 = bf16[1,32,12,2048]{3,2,0,1:T(8,128)(2,1)S(1)} all-to-all(bf16[1,32,12,2048]{3,2,0,1:T(8,128)(2,1)S(1)} %bitcast.122), channel_id=1, replica_groups=mesh['sp'=32,'tp'=8] {'sp'}, dimensions={1} | all-to-all | bytes 3145728 | tf_op jit(solution)/shard_map/all_to_all | solution.py:161
  144.3 6.2 %stack.2 = bf16[8,1,32,12,2048]{4,2,3,1,0:T(8,128)(2,1)} broadcast(bf16[32,12,2048]{2,0,1:T(8,128)(2,1)S(1)} %copy.81), dimensions={2,3,4} | broadcast | bytes 14155776 | tf_op jit(solution)/shard_map/stack | solution.py:163
  150.5 145.4 %all_to_all.30 = bf16[8,1,32,12,2048]{4,2,3,1,0:T(8,128)(2,1)S(1)} all-to-all(bf16[8,1,32,12,2048]{4,2,3,1,0:T(8,128)(2,1)} %stack.2), channel_id=1, replica_groups=mesh['sp'=32,'tp'=8] {'tp'}, dimensions={0} | all-to-all | bytes 25165824 | tf_op jit(solution)/shard_map/all_to_all | solution.py:163
  295.9 21.1 %copy.82 = bf16[1,32,8,12,2048]{4,3,2,1,0:T(8,128)(2,1)} copy(bf16[1,32,8,12,2048]{4,1,3,0,2:T(8,128)(2,1)S(1)} %bitcast.120) | data formatting | bytes 25165824 | tf_op jit(solution)/shard_map/reshape | solution.py:162
  317.1 20.0 %reshape.427 = bf16[3072,2048]{1,0:T(8,128)(2,1)} reshape(bf16[1,32,8,12,2048]{4,3,2,1,0:T(8,128)(2,1)} %copy.82) | data formatting | bytes 25165824 | tf_op jit(solution)/shard_map/reshape.52
  337.1 7.8 %fusion.12 = f32[3072,128]{1,0:T(8,128)S(1)} fusion(bf16[3072,2048]{1,0:T(8,128)(2,1)} %reshape.427, bf16[1,2048,128]{2,1,0:T(8,128)(2,1)S(1)} %copy-done.10), kind=kOutput, calls=%fused_computation.37 | convolution fusion | flops 1610612736 | bytes 14680064 | tf_op jit(solution)/shard_map/esd,edf->esf/dot_general | solution.py:166
  345.3 4.5 fusion
  349.8 44.3 %all-gather.3.cloned.1.call-done = bf16[3072,1024]{1,0:T(8,128)(2,1)} async-done(((bf16[3072,128]{1,0:T(8,128)(2,1)}), bf16[3072,1024]{1,0:T(8,128)(2,1)}) %all-gather.3.cloned.1.call-update) | async-done | bytes 6291472 | tf_op jit(solution)/shard_map/all_gather | solution.py:175
  394.1 5.7 %convolution_convert_fusion = bf16[3072,256]{1,0:T(8,128)(2,1)} fusion(bf16[3072,1024]{1,0:T(8,128)(2,1)} %all-gather.3.cloned.1.call-done, bf16[1,1024,256]{2,1,0:T(8,128)(2,1)S(1)} %copy-done), kind=kOutput, calls=%fused_computation.6 | convolution fusion | flops 1611399168 | bytes 8388608 | tf_op jit(solution)/shard_map/esf,efc->esc/dot_general | solution.py:173
  399.9 9.9 %all-to-all-start.3 = ((bf16[1,32,96,256]{3,2,0,1:T(8,128)(2,1)}), bf16[1,32,96,256]{3,2,0,1:T(8,128)(2,1)S(1)}, u32[]{:S(2)}, u32[]{:S(2)}) async-start(bf16[1,32,96,256]{3,2,0,1:T(8,128)(2,1)} %bitcast.125), calls=%async_computation.3 | async-start | bytes 3145728 | tf_op jit(solution)/shard_map/all_to_all | solution.py:179
  411.0 36.4 %all-to-all-done.3 = bf16[1,32,96,256]{3,2,0,1:T(8,128)(2,1)S(1)} async-done(((bf16[1,32,96,256]{3,2,0,1:T(8,128)(2,1)}), bf16[1,32,96,256]{3,2,0,1:T(8,128)(2,1)S(1)}, u32[]{:S(2)}, u32[]{:S(2)}) %all-to-all-start.3) | async-done | bytes 1572896 | tf_op jit(solution)/shard_map/all_to_all | solution.py:179
  447.4 5.3 %gather_fusion.1 = bf16[1536,256]{1,0:T(8,128)(2,1)} fusion(bf16[3072,256]{1,0:T(8,128)(2,1)S(1)} %bitcast.121, s32[2048]{0:T(1024)S(1)} %pad_clamp_fusion), kind=kCustom, calls=%fused_computation.1 | custom fusion | bytes 1579008 | tf_op jit(solution)/shard_map/gather | solution.py:187
  452.7 2.2 reshape.464
  454.9 4.2 multiply_reduce_fusion.1
  460.5 10.8 %all_to_all.31 = f32[8,1,1536]{2,1,0:T(1,128)S(1)} all-to-all(f32[8,1,1536]{2,1,0:T(1,128)S(1)} %broadcast_in_dim.77), channel_id=1, replica_groups=mesh['sp'=32,'tp'=8] {'tp'}, dimensions={0} | all-to-all | bytes 98304 | tf_op jit(solution)/shard_map/all_to_all | solution.py:29
  (101 shorter events, 26.2 us)
Async XLA Ops:
  6.5 387.6 %copy-start = (bf16[1,1024,256]{2,1,0:T(8,128)(2,1)S(1)}, bf16[1,1024,256]{2,1,0:T(8,128)(2,1)}, u32[]{:S(2)}) copy-start(bf16[1,1024,256]{2,1,0:T(8,128)(2,1)} %param.28) | copy-start | bytes 1572868
  6.5 18.0 %copy-start.5 = (s32[768]{0:T(1024)S(1)}, s32[768]{0:T(1024)}, u32[]{:S(2)}) copy-start(s32[768]{0:T(1024)} %param.19) | copy-start | bytes 9220
  6.5 18.8 %copy-start.3 = (bf16[768,64]{0,1:T(8,128)(2,1)S(1)}, bf16[768,64]{0,1:T(8,128)(2,1)}, u32[]{:S(2)}) copy-start(bf16[768,64]{0,1:T(8,128)(2,1)} %param.17) | copy-start | bytes 294916
  7.4 17.2 %collective-permute-start.1 = (s32[128]{0:T(128)S(1)}, s32[128]{0:T(128)S(1)}, u32[]{:S(2)}, u32[]{:S(2)}) collective-permute-start(s32[128]{0:T(128)S(1)} %get-tuple-element.16), channel_id=1, source_target_pairs={{0,8},{8,16},{16,24},{24,32},{32,40},{40,48},{48,56},{56,64},{64,7... | collective-permute-start | bytes 1544 | tf_op jit(solution)/shard_map/ppermute | solution.py:19
  11.3 13.3 %collective-permute-start.3 = (s32[128]{0:T(128)S(1)}, s32[128]{0:T(128)S(1)}, u32[]{:S(2)}, u32[]{:S(2)}) collective-permute-start(s32[128]{0:T(128)S(1)} %get-tuple-element.17), channel_id=1, source_target_pairs={{8,0},{16,8},{24,16},{32,24},{40,32},{48,40},{56,48},{64,56},{72,6... | collective-permute-start | bytes 1544 | tf_op jit(solution)/shard_map/ppermute | solution.py:22
  14.4 11.7 %copy-start.8 = (f32[2]{0:T(128)S(1)}, f32[2]{0:T(128)}, u32[]{:S(2)}) copy-start(f32[2]{0:T(128)} %param.20) | copy-start | bytes 28
  14.4 11.3 %collective-permute-start = (bf16[128,128]{0,1:T(8,128)(2,1)S(1)}, bf16[128,128]{0,1:T(8,128)(2,1)S(1)}, u32[]{:S(2)}, u32[]{:S(2)}) collective-permute-start(bf16[128,128]{0,1:T(8,128)(2,1)S(1)} %get-tuple-element.7), channel_id=1, source_target_pairs={{0,8},{8,16},{16,24},{24,32},{32,40},{40,48},{48,56},{56,64},{64,7... | collective-permute-start | bytes 98312 | tf_op jit(solution)/shard_map/ppermute | solution.py:19
  18.4 7.9 %collective-permute-start.2 = (bf16[128,128]{0,1:T(8,128)(2,1)S(1)}, bf16[128,128]{0,1:T(8,128)(2,1)S(1)}, u32[]{:S(2)}, u32[]{:S(2)}) collective-permute-start(bf16[128,128]{0,1:T(8,128)(2,1)S(1)} %get-tuple-element.8), channel_id=1, source_target_pairs={{8,0},{16,8},{24,16},{32,24},{40,32},{48,40},{56,48},{64,56},{72,6... | collective-permute-start | bytes 98312 | tf_op jit(solution)/shard_map/ppermute | solution.py:22
  25.7 1.6 copy-start.4
  29.7 26.6 %all-to-all-start = ((bf16[8,768,128]{1,2,0:T(8,128)(2,1)}), bf16[8,768,128]{1,2,0:T(8,128)(2,1)S(1)}, u32[]{:S(2)}, u32[]{:S(2)}) async-start(bf16[8,768,128]{1,2,0:T(8,128)(2,1)} %broadcast_in_dim.73), calls=%async_computation | async-start | bytes 3145728 | tf_op jit(solution)/shard_map/all_to_all | solution.py:29
  35.7 358.4 %all-gather.3.cloned.1.call-start = ((), (), s32[]{:S(2)}) async-start(), calls=%async_computation.5 | async-start | bytes 7077888 | tf_op jit(solution)/shard_map/all_gather | solution.py:175
  63.7 0.8 copy-start.6
  65.3 1.7 copy-start.1
  317.1 20.0 %copy-start.10 = (bf16[1,2048,128]{2,1,0:T(8,128)(2,1)S(1)}, bf16[1,2048,128]{2,1,0:T(8,128)(2,1)}, u32[]{:S(2)}) copy-start(bf16[1,2048,128]{2,1,0:T(8,128)(2,1)} %param.26) | copy-start | bytes 1572868
  337.1 8.2 %copy-start.2 = (bf16[3072,2048]{1,0:T(8,128)(2,1)S(1)}, bf16[3072,2048]{1,0:T(8,128)(2,1)}, u32[]{:S(2)}) copy-start(bf16[3072,2048]{1,0:T(8,128)(2,1)} %reshape.427) | copy-start | bytes 37748740
  337.1 8.2 %copy-start.11 = (bf16[1,2048,128]{2,1,0:T(8,128)(2,1)S(1)}, bf16[1,2048,128]{2,1,0:T(8,128)(2,1)}, u32[]{:S(2)}) copy-start(bf16[1,2048,128]{2,1,0:T(8,128)(2,1)} %param.27) | copy-start | bytes 1572868
  399.9 10.9 %copy-start.7 = (f32[768,2]{0,1:T(2,128)S(1)}, f32[768,2]{0,1:T(2,128)}, u32[]{:S(2)}) copy-start(f32[768,2]{0,1:T(2,128)} %param.25) | copy-start | bytes 18436
  399.9 47.5 %all-to-all-start.3 = ((bf16[1,32,96,256]{3,2,0,1:T(8,128)(2,1)}), bf16[1,32,96,256]{3,2,0,1:T(8,128)(2,1)S(1)}, u32[]{:S(2)}, u32[]{:S(2)}) async-start(bf16[1,32,96,256]{3,2,0,1:T(8,128)(2,1)} %bitcast.125), calls=%async_computation.3 | async-start | bytes 3145728 | tf_op jit(solution)/shard_map/all_to_all | solution.py:179
  452.7 18.6 %copy-start.9 = (f32[256]{0:T(256)S(1)}, f32[256]{0:T(256)}, u32[]{:S(2)}) copy-start(f32[256]{0:T(256)} %param.29) | copy-start | bytes 3076
Sparse Core Ops, SparseCore 0:
  349.9 44.1 all-gather.2
